TPU v7x, 32 devices: a whole 2x2x4 slice. The times are simulated.
32 devices in a mesh: grp: 2 (over x), ep: 16 (over z, y, core).
Axes of the slice: x: 2, y: 2, z: 4, core: 2. Of those that a mesh axis runs over, the one named last changes fastest.
Arguments:
- queries: bfloat16 [32, 8, 128], P(('grp', 'ep')), parts along dimension 0, may hold values from -400 to 400
- fresh_token_key: bfloat16 [32, 2, 128], P(('grp', 'ep')), parts along dimension 0, may hold values from -6 to 6
- value_new: bfloat16 [32, 2, 128], P(('grp', 'ep')), parts along dimension 0, may hold values from -6 to 6
- forget_logit: float32 [32, 8], P(('grp', 'ep')), parts along dimension 0, may hold values from -8 to 8
- cache_keys: bfloat16 [32, 2, 4096, 128], P(('grp', 'ep')), parts along dimension 0, may hold values from -12 to 12
- cache_values: bfloat16 [32, 2, 4096, 128], P(('grp', 'ep')), parts along dimension 0, may hold values from -6 to 6
- cache_cumlog: float32 [32, 8, 4096], P(('grp', 'ep')), parts along dimension 0, may hold values from -572 to 0
- lengths: int32 [32], P(('grp', 'ep')), parts along dimension 0, may hold values from 1024 to 4096
- residual: bfloat16 [32, 2048], P('grp', 'ep'), parts along dimension 0, may hold values from -6 to 6
- out_weight: bfloat16 [1024, 2048], P(None, 'ep'), may hold values from -0.1875 to 0.1875
- norm_gain: float32 [2048], replicated, may hold values from 0.1 to 1.9
- expert_gate: bfloat16 [16, 704, 2048], P('ep'), may hold values from -0.125 to 0.125
- expert_up: bfloat16 [16, 704, 2048], P('ep'), may hold values from -0.125 to 0.125
- expert_down: bfloat16 [16, 704, 2048], P('ep'), may hold values from -0.21875 to 0.21875
- shared_gate: bfloat16 [1408, 2048], P('ep'), may hold values from -0.125 to 0.125
- shared_up: bfloat16 [1408, 2048], P('ep'), may hold values from -0.125 to 0.125
- shared_down: bfloat16 [1408, 2048], P(None, 'ep'), may hold values from -0.15625 to 0.15625
- routes: int32 [32, 6], P('grp'), parts along dimension 0, may hold values from 0 to 15, all different within a row; in each aligned block of 16 rows (0 to 15, 16 to 31, ...) at most 12 rows name the same one
- route_scores: float32 [32, 6], P('grp'), parts along dimension 0, may hold values from 0.05 to 1
Outputs:
- updated: bfloat16 [32, 2048], P('grp', 'ep'), parts along dimension 0
There are 2 independent parts, one for each index of `grp`. A program takes and returns all parts, laid end to end along the dimension named above; an argument that names none is the same for every part. Nothing has to cross between parts.
Inputs may be any that keep to these rules, and one draw needn't show every extreme that they name: `routes`: each row names 6 different experts; no expert is named by more than 12 rows of a part, a bound that some block reaches.
All inputs are finite; a program needn't handle non-finite values.
Results may differ from a plain program's by a relative error of at most 0.0068.
Values may be sent and summed in bfloat16 or wider, within the bound.
No kernel may reach another device: no remote copies, remote signals or barrier semaphores. Data moves between devices by JAX's collectives and lax.ppermute only.
A program may use at most 64 MiB of HBM per device.

v0:
```python
import jax
import jax.numpy as jnp
from jax import lax
from jax.sharding import PartitionSpec as P

CAP = 12
norm_eps = 1e-06
routed_scale = 2.5
contract_last = (((1,), (1,)), ((), ()))


def expert_hidden(row_block, gate_matrix, up_matrix):
    gate_part = lax.dot_general(
        row_block, gate_matrix, contract_last, preferred_element_type=jnp.float32
    )
    up_part = lax.dot_general(
        row_block, up_matrix, contract_last, preferred_element_type=jnp.float32
    )
    return (jax.nn.silu(gate_part) * up_part).astype(jnp.bfloat16)


def attention(
    queries,
    fresh_token_key,
    value_new,
    forget_logit,
    cache_keys,
    cache_values,
    cache_cumlog,
    lengths,
):
    batch_rows, head_count, head_size = queries.shape
    key_heads = cache_keys.shape[1]
    cache_span = cache_keys.shape[2]
    groups = head_count // key_heads
    inv_root = head_size ** (-0.5)
    grouped_heads = queries.reshape(batch_rows, key_heads, groups, head_size)
    scores = (
        jnp.einsum(
            "bkgd,bkpd->bkgp", grouped_heads, cache_keys, preferred_element_type=jnp.float32
        ).reshape(batch_rows, head_count, cache_span)
        * inv_root
    )
    positions = lax.broadcasted_iota(jnp.int32, (1, 1, cache_span), 2)
    last_pos = (lengths - 1)[:, None, None]
    latest = jnp.sum(jnp.where(positions == last_pos, cache_cumlog, 0.0), axis=2)
    log_gate = jax.nn.log_sigmoid(forget_logit)
    scores = scores + (latest + log_gate)[:, :, None] - cache_cumlog
    visible = positions < lengths[:, None, None]
    scores = jnp.where(visible, scores, -jnp.inf)
    own_score = (
        jnp.einsum(
            "tiuh,tih->tiu", grouped_heads, fresh_token_key, preferred_element_type=jnp.float32
        ).reshape(batch_rows, head_count)
        * inv_root
    )
    top_score = jnp.maximum(jnp.max(scores, axis=2), own_score)
    weights = jnp.where(visible, jnp.exp(scores - top_score[:, :, None]), 0.0)
    own_weight = jnp.exp(own_score - top_score)
    denominator = jnp.sum(weights, axis=2) + own_weight
    weighted = jnp.einsum(
        "bkgp,bkpd->bkgd",
        weights.astype(jnp.bfloat16).reshape(batch_rows, key_heads, groups, cache_span),
        cache_values,
        preferred_element_type=jnp.float32,
    )
    own_rounded = lax.optimization_barrier(own_weight.astype(jnp.bfloat16)).astype(jnp.float32)
    own_value = jnp.repeat(value_new, groups, axis=1).astype(jnp.float32)
    numerator = (
        weighted.reshape(batch_rows, head_count, head_size) + own_rounded[:, :, None] * own_value
    )
    return (
        (numerator / denominator[:, :, None])
        .astype(jnp.bfloat16)
        .reshape(batch_rows, head_count * head_size)
    )


def on_device(
    queries,
    fresh_token_key,
    value_new,
    forget_logit,
    cache_keys,
    cache_values,
    cache_cumlog,
    lengths,
    residual,
    out_weight,
    norm_gain,
    expert_gate,
    expert_up,
    expert_down,
    shared_gate,
    shared_up,
    shared_down,
    routes,
    route_scores,
):
    attended = attention(
        queries,
        fresh_token_key,
        value_new,
        forget_logit,
        cache_keys,
        cache_values,
        cache_cumlog,
        lengths,
    )
    mixed = jnp.dot(
        lax.all_gather(attended, "ep", axis=0, tiled=True),
        out_weight,
        preferred_element_type=jnp.float32,
    )
    stream = (residual.astype(jnp.float32) + mixed).astype(jnp.bfloat16)
    full_rows = lax.all_gather(stream, "ep", axis=1, tiled=True)
    rows_wide = full_rows.astype(jnp.float32)
    inv_rms = lax.rsqrt(jnp.mean(rows_wide * rows_wide, axis=1, keepdims=True) + norm_eps)
    normed = (rows_wide * inv_rms * norm_gain).astype(jnp.bfloat16)
    gate_weights = route_scores / jnp.sum(route_scores, axis=1, keepdims=True) * routed_scale
    shared_mid = expert_hidden(normed, shared_gate, shared_up)
    my_expert = lax.axis_index("ep")
    expert_hits = routes == my_expert
    is_member = jnp.sum(expert_hits.astype(jnp.int32), axis=1)
    slot_rank = jnp.cumsum(is_member) - 1
    slot_ids = lax.broadcasted_iota(jnp.int32, (CAP, 1), 0)
    selector = (is_member[None, :] == 1) & (slot_rank[None, :] == slot_ids)
    picked = jnp.dot(
        selector.astype(jnp.bfloat16), normed, preferred_element_type=jnp.float32
    ).astype(jnp.bfloat16)
    hidden = expert_hidden(picked, expert_gate[0], expert_up[0])
    expert_out = jnp.dot(hidden, expert_down[0], preferred_element_type=jnp.float32).astype(
        jnp.bfloat16
    )
    received = lax.all_to_all(expert_out[None], "ep", split_axis=2, concat_axis=0, tiled=True)
    expert_count = received.shape[0]
    expert_ids = lax.broadcasted_iota(jnp.int32, (1, 1, expert_count), 2)
    all_hits = routes[:, :, None] == expert_ids
    membership = jnp.sum(all_hits.astype(jnp.int32), axis=1)
    share_all = jnp.sum(jnp.where(all_hits, gate_weights[:, :, None], 0.0), axis=1)
    rank_all = jnp.cumsum(membership, axis=0) - 1
    slot_grid = lax.broadcasted_iota(jnp.int32, (1, 1, CAP), 2)
    slot_mask = (membership[:, :, None] == 1) & (rank_all[:, :, None] == slot_grid)
    combiner = jnp.where(slot_mask, share_all[:, :, None], 0.0).reshape(
        routes.shape[0], expert_count * CAP
    )
    flat_slots = received.reshape(expert_count * CAP, received.shape[2]).astype(jnp.float32)
    routed_part = jnp.dot(combiner, flat_slots, precision=lax.Precision.HIGHEST)
    shared_part = jnp.dot(
        lax.all_gather(shared_mid, "ep", axis=1, tiled=True),
        shared_down,
        preferred_element_type=jnp.float32,
    )
    return (stream.astype(jnp.float32) + routed_part + shared_part).astype(jnp.bfloat16)


def solution(mesh):
    placed = (
        P(("grp", "ep"), None, None),
        P(("grp", "ep"), None, None),
        P(("grp", "ep"), None, None),
        P(("grp", "ep"), None),
        P(("grp", "ep"), None, None, None),
        P(("grp", "ep"), None, None, None),
        P(("grp", "ep"), None, None),
        P(("grp", "ep")),
        P("grp", "ep"),
        P(None, "ep"),
        P(),
        P("ep", None, None),
        P("ep", None, None),
        P("ep", None, None),
        P("ep", None),
        P("ep", None),
        P(None, "ep"),
        P("grp", None),
        P("grp", None),
    )
    return jax.shard_map(
        on_device, mesh=mesh, in_specs=placed, out_specs=P("grp", "ep"), check_vma=False
    )
```

profile of v0, /device:TPU:0, one launch (start us, length us, event | category | flops | bytes accessed | tf_op | source)
XLA Modules:
  0.0 110.7 jit_solution(4193211708962261572)
XLA Ops:
  0.0 0.9 fusion.47
  1.8 0.7 convert_reduce_fusion.1
  2.5 0.7 bitcast_convert_fusion
  3.3 0.1 add_reduce_fusion
  3.4 2.3 %convolution_multiply_fusion = f32[2,4,4096]{2,1,0:T(4,128)S(1)} fusion(bf16[2,4,128]{2,1,0:T(4,128)(2,1)} %bitcast.100, bf16[1,2,4096,128]{3,2,1,0:T(8,128)(2,1)} %param.23), kind=kOutput, calls=%fused_computation | convolution fusion | flops 8421376 | bytes 2230272 | tf_op jit(solution)/shard_map/bkgd,bkpd->bkgp/dot_general | solution.py:39
  5.7 1.1 select_reduce_fusion
  6.8 0.7 fusion.52
  7.5 1.1 %fusion.59 = (f32[8]{0:T(128)S(1)}, f32[1,8,4096]{2,1,0:T(8,128)S(1)}) fusion(f32[1,8,4096]{2,1,0:T(8,128)} %param.25, f32[1,8,4096]{2,1,0:T(8,128)S(1)} %mul.103, f32[8]{0:T(128)S(1)} %fusion.52, pred[4096]{0:T(1024)(128)(4,1)S(1)} %iota_compare_fusion.3), kind=kLoop, calls=%fused_computation.78 | loop fusion | flops 131064 | bytes 397376 | tf_op jit(solution)/shard_map/reduce_max | solution.py:57
  8.6 0.2 fusion.34
  8.9 2.0 %fusion.12 = f32[2,4,128]{2,1,0:T(4,128)S(1)} fusion(bf16[2,4,4096]{2,1,0:T(4,128)(2,1)S(1)} %reshape.347, bf16[1,2,4096,128]{3,2,1,0:T(8,128)(2,1)} %param.24), kind=kOutput, calls=%fused_computation.10 | convolution fusion | flops 8388608 | bytes 2166784 | tf_op jit(solution)/shard_map/bkgp,bkpd->bkgd/dot_general | solution.py:61
  11.1 23.3 %all-gather = bf16[16,1,1024]{2,1,0:T(2,128)(2,1)S(1)} all-gather(bf16[1,1,1024]{2,1,0:T(2,128)(2,1)S(1)} %convert_bitcast_fusion), channel_id=1, replica_groups=mesh['grp'=2,'ep'=16] {'ep'}, dimensions={0}, use_global_device_ids=true | all-gather | bytes 34816 | tf_op jit(solution)/shard_map/all_gather | solution.py:111
  34.4 0.2 fusion.22
  34.5 17.6 %all_gather.10 = bf16[16,2048]{1,0:T(8,128)(2,1)S(1)} all-gather(bf16[16,128]{1,0:T(8,128)(2,1)S(1)} %fusion.22), channel_id=1, replica_groups=mesh['grp'=2,'ep'=16] {'ep'}, dimensions={1}, use_global_device_ids=true | all-gather | bytes 69632 | tf_op jit(solution)/shard_map/all_gather | solution.py:116
  52.1 0.1 fusion.28
  52.2 0.2 convolution_convert_fusion
  52.5 2.7 %fusion.4 = f32[12,704]{1,0:T(8,128)S(1)} fusion(bf16[12,2048]{1,0:T(8,128)(2,1)S(1)} %convolution_convert_fusion, bf16[1,704,2048]{2,1,0:T(8,128)(2,1)} %param.30), kind=kOutput, calls=%fused_computation.5 | convolution fusion | flops 34603008 | bytes 2966528 | tf_op jit(solution)/shard_map/dot_general | solution.py:13
  55.1 3.5 %fusion.9 = bf16[1,12,2048]{2,1,0:T(8,128)(2,1)S(1)} fusion(bf16[1,704,2048]{2,1,0:T(8,128)(2,1)S(1)} %copy-done, bf16[12,2048]{1,0:T(8,128)(2,1)S(1)} %convolution_convert_fusion, bf16[1,704,2048]{2,1,0:T(8,128)(2,1)} %param.31, f32[12,704]{1,0:T(8,128)S(1)} %fusion.4), kind=kOutput, calls=%fused_computation.9 | convolution fusion | flops 69281280 | bytes 5899264 | tf_op jit(solution)/shard_map/dot_general | solution.py:132
  58.6 2.0 %copy.42 = bf16[1,12,2048]{1,0,2:T(2,128)(2,1)} copy(bf16[1,12,2048]{2,1,0:T(8,128)(2,1)S(1)} %fusion.9) | data formatting | bytes 98304 | tf_op jit(solution)/shard_map/broadcast_in_dim | solution.py:135
  60.7 0.5 broadcast.203
  61.2 12.6 %reduce.5 = bf16[2048,12]{1,0:T(8,128)(2,1)S(1)} reduce(bf16[2048,1,12]{2,1,0:T(2,128)(2,1)} %bitcast.91, bf16[]{:T(256)} %broadcast.203), dimensions={1}, to_apply=%bitcast.76.reduce_sub_computation | reduce | bytes 98306
  73.8 1.6 %reshape.361 = bf16[16,2,768]{2,1,0:T(2,128)(2,1)} reshape(bf16[2048,12]{1,0:T(8,128)(2,1)S(1)} %reduce.5) | data formatting | bytes 98304
  75.3 3.5 %all-to-all-start = ((bf16[16,2,768]{2,1,0:T(2,128)(2,1)}), bf16[16,2,768]{2,1,0:T(2,128)(2,1)S(1)}, u32[]{:S(2)}, u32[]{:S(2)}) async-start(bf16[16,2,768]{2,1,0:T(2,128)(2,1)} %reshape.361), calls=%async_computation | async-start | bytes 98304 | tf_op jit(solution)/shard_map/all_to_all | solution.py:135
  79.1 1.2 %fusion.56 = f32[16,88]{1,0:T(8,128)S(1)} fusion(bf16[88,2048]{1,0:T(8,128)(2,1)} %param.33, bf16[16,2048]{1,0:T(8,128)(2,1)S(1)} %all_gather.10, f32[2048]{0:T(1024)S(1)} %copy-done.2, f32[16]{0:T(128)S(1)} %add_rsqrt_fusion), kind=kOutput, calls=%fused_computation.77 | convolution fusion | flops 5898240 | bytes 439872 | tf_op jit(solution)/shard_map/dot_general | solution.py:13
  80.3 1.2 %fusion.25 = bf16[1,88,16]{1,2,0:T(8,128)(2,1)S(1)} fusion(bf16[88,2048]{1,0:T(8,128)(2,1)} %param.34, f32[16,88]{1,0:T(8,128)S(1)} %fusion.56, bf16[16,2048]{1,0:T(8,128)(2,1)S(1)} %all_gather.10, f32[2048]{0:T(1024)S(1)} %copy-done.2, f32[16]{0:T(128)S(1)} %add_rsqrt_fusion), kind=kOutput, calls=%fused_computation.22 | convolution fusion | flops 5906688 | bytes 442688 | tf_op jit(solution)/shard_map/dot_general | solution.py:16
  81.6 21.8 %all-gather.1 = bf16[16,88,16]{1,2,0:T(8,128)(2,1)S(1)} all-gather(bf16[1,88,16]{1,2,0:T(8,128)(2,1)S(1)} %fusion.25), channel_id=1, replica_groups=mesh['grp'=2,'ep'=16] {'ep'}, dimensions={0}, use_global_device_ids=true | all-gather | bytes 47872 | tf_op jit(solution)/shard_map/all_gather | solution.py:150
  103.4 0.1 reshape.357
  103.6 1.1 %fusion.60 = f32[16,128]{1,0:T(8,128)S(1)} fusion(bf16[1408,16]{0,1:T(8,128)(2,1)S(1)} %reshape.357, bf16[1408,128]{1,0:T(8,128)(2,1)} %param.35), kind=kOutput, calls=%fused_computation.79 | convolution fusion | flops 5767168 | bytes 413696 | tf_op jit(solution)/shard_map/dot_general | solution.py:149
  104.7 0.2 fusion.32
  104.9 0.1 select_n.39
  105.0 2.5 %reshape.362 = bf16[2048,1,12]{2,1,0:T(2,128)(2,1)} reshape(bf16[16,2,768]{2,1,0:T(2,128)(2,1)S(1)} %all-to-all-done) | data formatting | bytes 98304
  107.5 2.3 %copy.43 = bf16[1,12,2048]{2,1,0:T(8,128)(2,1)S(1)} copy(bf16[1,12,2048]{1,0,2:T(2,128)(2,1)} %bitcast.92) | data formatting | bytes 98304 | tf_op jit(solution)/shard_map/all_to_all | solution.py:135
  109.9 0.8 fusion.23
  (44 shorter events, 1.0 us)
Async XLA Ops:
  0.0 55.1 %copy-start = (bf16[1,704,2048]{2,1,0:T(8,128)(2,1)S(1)}, bf16[1,704,2048]{2,1,0:T(8,128)(2,1)}, u32[]{:S(2)}) copy-start(bf16[1,704,2048]{2,1,0:T(8,128)(2,1)} %param.32) | copy-start | bytes 8650756
  0.0 34.4 %copy-start.1 = (bf16[1024,128]{1,0:T(8,128)(2,1)S(1)}, bf16[1024,128]{1,0:T(8,128)(2,1)}, u32[]{:S(2)}) copy-start(bf16[1024,128]{1,0:T(8,128)(2,1)} %param.28) | copy-start | bytes 786436
  0.0 34.4 %copy-start.5 = (bf16[16,128]{1,0:T(8,128)(2,1)S(1)}, bf16[16,128]{1,0:T(8,128)(2,1)}, u32[]{:S(2)}) copy-start(bf16[16,128]{1,0:T(8,128)(2,1)} %param.27) | copy-start | bytes 12292
  3.4 48.8 %copy-start.2 = (f32[2048]{0:T(1024)S(1)}, f32[2048]{0:T(1024)}, u32[]{:S(2)}) copy-start(f32[2048]{0:T(1024)} %param.29) | copy-start | bytes 24580
  58.6 20.2 %copy-start.3 = (s32[16,6]{0,1:T(8,128)S(1)}, s32[16,6]{0,1:T(8,128)}, u32[]{:S(2)}) copy-start(s32[16,6]{0,1:T(8,128)} %param.36) | copy-start | bytes 1156
  58.6 20.3 %copy-start.4 = (f32[16,6]{0,1:T(8,128)S(1)}, f32[16,6]{0,1:T(8,128)}, u32[]{:S(2)}) copy-start(f32[16,6]{0,1:T(8,128)} %param.37) | copy-start | bytes 1156
  75.3 29.7 %all-to-all-start = ((bf16[16,2,768]{2,1,0:T(2,128)(2,1)}), bf16[16,2,768]{2,1,0:T(2,128)(2,1)S(1)}, u32[]{:S(2)}, u32[]{:S(2)}) async-start(bf16[16,2,768]{2,1,0:T(2,128)(2,1)} %reshape.361), calls=%async_computation | async-start | bytes 98304 | tf_op jit(solution)/shard_map/all_to_all | solution.py:135
where the time goes:
time: 111 us
  blocking collectives  62.7 us (56%)
  other arithmetic  17.8 us (16%)
  matrix products  16.1 us (15%)
  local copies, waits for them, and re-layouts  9.72 us (9%)
  starting transfers between devices  3.5 us (3%)
    all_gather x1, blocking collectives, on_device(): lax.all_gather(attended, 'ep', axis=0, tiled=True)  23.3 us
    all_gather x1, blocking collectives, on_device(): lax.all_gather(shared_mid, 'ep', axis=1, tiled=True)  21.8 us
    all_gather x1, blocking collectives, on_device(): full_rows = lax.all_gather(stream, 'ep', axis=1, tiled=True)  17.6 us
    unnamed x2, other arithmetic  12.6 us
    unnamed x17, local copies, waits for them, and re-layouts  4.7 us
    dot_general x2, matrix products, expert_hidden(): lax.dot_general(row_block, gate_matrix, contract_last, preferred_element_...  3.89 us
    all_to_all x1, starting transfers between devices, on_device(): lax.all_to_all(expert_out[None], 'ep', split_axis=2, concat_axis=0, tiled...  3.5 us
    dot_general x1, matrix products, on_device(): jnp.dot(hidden, expert_down[0], preferred_element_type=jnp.float32)  3.49 us
  transfers between devices with their start and end apart: 1, of which 0 were waited for; matrix products, arithmetic and copies ran while one was open for 4% of the time, Pallas kernels for 0%

commit v1 on v0

--- a/solution.py
+++ b/solution.py
@@ -132,7 +132,11 @@
     expert_out = jnp.dot(hidden, expert_down[0], preferred_element_type=jnp.float32).astype(
         jnp.bfloat16
     )
-    received = lax.all_to_all(expert_out[None], "ep", split_axis=2, concat_axis=0, tiled=True)
+    part = expert_out[None]
+    size = lax.axis_size("ep")
+    blocks = jnp.stack(jnp.split(part, size, axis=2), axis=0)
+    blocks = lax.all_to_all(blocks, "ep", split_axis=0, concat_axis=0)
+    received = jnp.concatenate(blocks, axis=0)
     expert_count = received.shape[0]
     expert_ids = lax.broadcasted_iota(jnp.int32, (1, 1, expert_count), 2)
     all_hits = routes[:, :, None] == expert_ids

time: 111 us -> 96.8 us (0.87)
  other arithmetic: 17.8 us -> 3.89 us
    unnamed x2 -> x1, other arithmetic: 12.6 us -> 0.03 us
    unnamed x17 -> x32, local copies, waits for them, and re-layouts: 4.7 us -> 9.07 us
    all_to_all x3 -> x0, local copies, waits for them, and re-layouts: 2.35 us -> none  [on_device(): lax.all_to_all(expert_out[None], 'ep', split_axis=2, concat_axis=0, tiled...]
    broadcast_in_dim x1 -> x0, local copies, waits for them, and re-layouts: 2.04 us -> none  [on_device(): expert_out[None]]
  transfers between devices with their start and end apart: 1 -> 1, of which waited for: 0 -> 0; matrix products, arithmetic and copies ran while one was open for 4% -> 3% of each run, Pallas kernels for 0% -> 0%
where the time goes in v1:
time: 96.8 us; the launch traced here: 96.4 us
  blocking collectives  62.7 us (65%)
  matrix products  15.2 us (16%)
  local copies, waits for them, and re-layouts  10.3 us (11%)
  other arithmetic  3.89 us (4%)
  starting transfers between devices  3.5 us (4%)
    all_gather x1, blocking collectives, on_device(): lax.all_gather(attended, 'ep', axis=0, tiled=True)  23.3 us
    all_gather x1, blocking collectives, on_device(): lax.all_gather(shared_mid, 'ep', axis=1, tiled=True)  21.8 us
    all_gather x1, blocking collectives, on_device(): full_rows = lax.all_gather(stream, 'ep', axis=1, tiled=True)  17.6 us
    unnamed x32, local copies, waits for them, and re-layouts  9.07 us
    dot_general x2, matrix products, expert_hidden(): lax.dot_general(row_block, gate_matrix, contract_last, preferred_element_...  3.89 us
    dot_general x1, matrix products, on_device(): jnp.dot(hidden, expert_down[0], preferred_element_type=jnp.float32)  3.53 us
    all_to_all x1, starting transfers between devices, on_device(): blocks = lax.all_to_all(blocks, 'ep', split_axis=0, concat_axis=0)  3.5 us
    dot_general x1, matrix products, attention(): jnp.einsum('bkgd,bkpd->bkgp', grouped_heads, cache_keys, preferred_elemen...  2.27 us
  transfers between devices with their start and end apart: 1, of which 0 were waited for; matrix products, arithmetic and copies ran while one was open for 3% of the time, Pallas kernels for 0%

profile of v1, /device:TPU:0, one launch (start us, length us, event | category | flops | bytes accessed | tf_op | source)
XLA Modules:
  0.0 96.4 jit_solution(13771426093455704900)
XLA Ops:
  0.0 1.0 fusion.47
  1.1 2.3 %convolution_multiply_fusion = f32[2,4,4096]{2,1,0:T(4,128)S(1)} fusion(bf16[2,4,128]{2,1,0:T(4,128)(2,1)} %bitcast.148, bf16[1,2,4096,128]{3,2,1,0:T(8,128)(2,1)} %param.23), kind=kOutput, calls=%fused_computation | convolution fusion | flops 8421376 | bytes 2230272 | tf_op jit(solution)/shard_map/bkgd,bkpd->bkgp/dot_general | solution.py:39
  4.2 1.1 %select_reduce_fusion = f32[8]{0:T(128)S(1)} fusion(f32[1,8,4096]{2,1,0:T(8,128)} %param.25, pred[4096]{0:T(1024)(128)(4,1)S(1)} %iota_compare_fusion.2), kind=kLoop, calls=%fused_computation.31 | loop fusion | flops 65528 | bytes 135200 | tf_op jit(solution)/shard_map/reduce_sum | solution.py:46
  5.2 0.7 fusion.52
  5.9 1.1 %fusion.59 = (f32[8]{0:T(128)S(1)}, f32[1,8,4096]{2,1,0:T(8,128)S(1)}) fusion(f32[1,8,4096]{2,1,0:T(8,128)} %param.25, f32[1,8,4096]{2,1,0:T(8,128)S(1)} %mul.103, f32[8]{0:T(128)S(1)} %fusion.52, pred[4096]{0:T(1024)(128)(4,1)S(1)} %iota_compare_fusion.3), kind=kLoop, calls=%fused_computation.109 | loop fusion | flops 131064 | bytes 397376 | tf_op jit(solution)/shard_map/reduce_max | solution.py:57
  7.3 2.0 %fusion.12 = f32[2,4,128]{2,1,0:T(4,128)S(1)} fusion(bf16[2,4,4096]{2,1,0:T(4,128)(2,1)S(1)} %reshape.343, bf16[1,2,4096,128]{3,2,1,0:T(8,128)(2,1)} %param.24), kind=kOutput, calls=%fused_computation.10 | convolution fusion | flops 8388608 | bytes 2166784 | tf_op jit(solution)/shard_map/bkgp,bkpd->bkgd/dot_general | solution.py:61
  9.5 23.3 %all-gather = bf16[16,1,1024]{2,1,0:T(2,128)(2,1)S(1)} all-gather(bf16[1,1,1024]{2,1,0:T(2,128)(2,1)S(1)} %convert_bitcast_fusion), channel_id=1, replica_groups=mesh['grp'=2,'ep'=16] {'ep'}, dimensions={0}, use_global_device_ids=true | all-gather | bytes 34816 | tf_op jit(solution)/shard_map/all_gather | solution.py:111
  33.0 17.6 %all_gather.10 = bf16[16,2048]{1,0:T(8,128)(2,1)S(1)} all-gather(bf16[16,128]{1,0:T(8,128)(2,1)S(1)} %fusion.22), channel_id=1, replica_groups=mesh['grp'=2,'ep'=16] {'ep'}, dimensions={1}, use_global_device_ids=true | all-gather | bytes 69632 | tf_op jit(solution)/shard_map/all_gather | solution.py:116
  51.2 2.7 %fusion.4 = f32[12,704]{1,0:T(8,128)S(1)} fusion(bf16[12,2048]{1,0:T(8,128)(2,1)S(1)} %convolution_convert_fusion, bf16[1,704,2048]{2,1,0:T(8,128)(2,1)} %param.30), kind=kOutput, calls=%fused_computation.5 | convolution fusion | flops 34603008 | bytes 2966528 | tf_op jit(solution)/shard_map/dot_general | solution.py:13
  53.9 3.5 %fusion.9 = bf16[1,12,2048]{2,1,0:T(8,128)(2,1)S(1)} fusion(bf16[1,704,2048]{2,1,0:T(8,128)(2,1)S(1)} %copy-done, bf16[12,2048]{1,0:T(8,128)(2,1)S(1)} %convolution_convert_fusion, bf16[1,704,2048]{2,1,0:T(8,128)(2,1)} %param.31, f32[12,704]{1,0:T(8,128)S(1)} %fusion.4), kind=kOutput, calls=%fused_computation.9 | convolution fusion | flops 69281280 | bytes 5899264 | tf_op jit(solution)/shard_map/dot_general | solution.py:132
  57.4 0.6 constant_dynamic-update-slice_fusion.15
  58.0 0.6 constant_dynamic-update-slice_fusion.14
  58.6 0.6 constant_dynamic-update-slice_fusion.13
  59.2 0.6 constant_dynamic-update-slice_fusion.12
  59.8 0.6 constant_dynamic-update-slice_fusion.11
  60.4 0.6 constant_dynamic-update-slice_fusion.10
  61.0 0.6 constant_dynamic-update-slice_fusion.9
  61.6 0.6 constant_dynamic-update-slice_fusion.8
  62.2 0.6 constant_dynamic-update-slice_fusion.7
  62.7 0.6 constant_dynamic-update-slice_fusion.6
  63.3 0.6 constant_dynamic-update-slice_fusion.5
  63.9 0.6 constant_dynamic-update-slice_fusion.4
  64.5 0.6 constant_dynamic-update-slice_fusion.3
  65.1 0.6 constant_dynamic-update-slice_fusion.2
  65.7 0.6 constant_dynamic-update-slice_fusion.1
  66.3 0.6 constant_dynamic-update-slice_fusion
  66.9 3.5 %all-to-all-start = ((bf16[16,1,12,128]{3,2,1,0:T(8,128)(2,1)}), bf16[16,1,12,128]{3,2,1,0:T(8,128)(2,1)S(1)}, u32[]{:S(2)}, u32[]{:S(2)}) async-start(bf16[16,1,12,128]{3,2,1,0:T(8,128)(2,1)} %constant_dynamic-update-slice_fusion), calls=%async_computation | async-start | bytes 131072 | tf_op jit(solution)/shard_map/all_to_all | solution.py:138
  70.5 1.2 %fusion.56 = f32[16,88]{1,0:T(8,128)S(1)} fusion(bf16[88,2048]{1,0:T(8,128)(2,1)} %param.33, bf16[16,2048]{1,0:T(8,128)(2,1)S(1)} %all_gather.10, f32[2048]{0:T(1024)S(1)} %copy-done.3, f32[16]{0:T(128)S(1)} %add_rsqrt_fusion), kind=kOutput, calls=%fused_computation.108 | convolution fusion | flops 5898240 | bytes 439872 | tf_op jit(solution)/shard_map/dot_general | solution.py:13
  71.8 0.3 fusion.25
  72.0 21.8 %all-gather.1 = bf16[16,88,16]{1,2,0:T(8,128)(2,1)S(1)} all-gather(bf16[1,88,16]{1,2,0:T(8,128)(2,1)S(1)} %fusion.25), channel_id=1, replica_groups=mesh['grp'=2,'ep'=16] {'ep'}, dimensions={0}, use_global_device_ids=true | all-gather | bytes 47872 | tf_op jit(solution)/shard_map/all_gather | solution.py:154
  94.2 1.2 %fusion.60 = f32[16,128]{1,0:T(8,128)S(1)} fusion(bf16[1408,16]{0,1:T(8,128)(2,1)S(1)} %reshape.352, bf16[1408,128]{1,0:T(8,128)(2,1)} %param.35), kind=kOutput, calls=%fused_computation.110 | convolution fusion | flops 5767168 | bytes 413696 | tf_op jit(solution)/shard_map/dot_general | solution.py:153
  95.6 0.8 fusion.23
  (55 shorter events, 2.2 us)
Async XLA Ops:
  0.0 53.8 %copy-start = (bf16[1,704,2048]{2,1,0:T(8,128)(2,1)S(1)}, bf16[1,704,2048]{2,1,0:T(8,128)(2,1)}, u32[]{:S(2)}) copy-start(bf16[1,704,2048]{2,1,0:T(8,128)(2,1)} %param.32) | copy-start | bytes 8650756
  0.0 7.3 %copy-start.7 = (bf16[1,2,128]{2,1,0:T(2,128)(2,1)S(1)}, bf16[1,2,128]{2,1,0:T(2,128)(2,1)}, u32[]{:S(2)}) copy-start(bf16[1,2,128]{2,1,0:T(2,128)(2,1)} %param.21) | copy-start | bytes 1540
  0.0 32.8 %copy-start.2 = (bf16[1024,128]{1,0:T(8,128)(2,1)S(1)}, bf16[1024,128]{1,0:T(8,128)(2,1)}, u32[]{:S(2)}) copy-start(bf16[1024,128]{1,0:T(8,128)(2,1)} %param.28) | copy-start | bytes 786436
  0.0 32.8 %copy-start.6 = (bf16[16,128]{1,0:T(8,128)(2,1)S(1)}, bf16[16,128]{1,0:T(8,128)(2,1)}, u32[]{:S(2)}) copy-start(bf16[16,128]{1,0:T(8,128)(2,1)} %param.27) | copy-start | bytes 12292
  1.1 49.5 %copy-start.4 = (s32[16,6]{0,1:T(8,128)S(1)}, s32[16,6]{0,1:T(8,128)}, u32[]{:S(2)}) copy-start(s32[16,6]{0,1:T(8,128)} %param.36) | copy-start | bytes 1156
  1.1 49.8 %copy-start.3 = (f32[2048]{0:T(1024)S(1)}, f32[2048]{0:T(1024)}, u32[]{:S(2)}) copy-start(f32[2048]{0:T(1024)} %param.29) | copy-start | bytes 24580
  53.8 17.9 %copy-start.1 = (bf16[88,2048]{1,0:T(8,128)(2,1)S(1)}, bf16[88,2048]{1,0:T(8,128)(2,1)}, u32[]{:S(2)}) copy-start(bf16[88,2048]{1,0:T(8,128)(2,1)} %param.34) | copy-start | bytes 1081348
  53.8 40.2 %copy-start.5 = (f32[16,6]{0,1:T(8,128)S(1)}, f32[16,6]{0,1:T(8,128)}, u32[]{:S(2)}) copy-start(f32[16,6]{0,1:T(8,128)} %param.37) | copy-start | bytes 1156
  66.9 28.7 %all-to-all-start = ((bf16[16,1,12,128]{3,2,1,0:T(8,128)(2,1)}), bf16[16,1,12,128]{3,2,1,0:T(8,128)(2,1)S(1)}, u32[]{:S(2)}, u32[]{:S(2)}) async-start(bf16[16,1,12,128]{3,2,1,0:T(8,128)(2,1)} %constant_dynamic-update-slice_fusion), calls=%async_computation | async-start | bytes 131072 | tf_op jit(solution)/shard_map/all_to_all | solution.py:138
